TPU v7x, 32 devices: a whole 2x2x4 slice. The times are simulated.
32 devices in a mesh: grp: 2 (over y), sp: 4 (over z), tp: 4 (over x, core).
Axes of the slice: x: 2, y: 2, z: 4, core: 2. Of those that a mesh axis runs over, the one named last changes fastest.
Arguments:
- tokens: bfloat16 [1280, 2048], P(('grp', 'sp')), parts along dimension 0, may hold values from -6 to 6
- norm_gain: float32 [2048], replicated, may hold values from 0.6 to 5
- query_weight: bfloat16 [2048, 2048], P('sp', 'tp')
- key_weight: bfloat16 [2048, 512], P('sp', 'tp')
- value_weight: bfloat16 [2048, 512], P('sp', 'tp'), may hold values from -0.125 to 0.125
- map_lambda: float32 [16], P('tp'), may hold values from 0.3 to 0.8
- head_gain: float32 [16, 128], P('tp'), may hold values from 0.1 to 1.9
- attn_out_weight: bfloat16 [2048, 2048], P('tp', 'sp'), may hold values from -0.125 to 0.125
- pool_out_weight: bfloat16 [2048, 2048], P('tp', 'sp'), may hold values from -0.09375 to 0.09375
Outputs:
- mixed_rows: bfloat16 [1280, 2048], P(('grp', 'sp', 'tp')), parts along dimension 0
- log_totals: float32 [2, 16, 1280], P(None, 'tp', ('grp', 'sp')), parts along dimension 2
There are 2 independent parts, one for each index of `grp`. A program takes and returns all parts, laid end to end along the dimension named above; an argument that names none is the same for every part. Nothing has to cross between parts.
All inputs are finite; a program needn't handle non-finite values.
Results may differ from a plain program's by a relative error of at most 0.013.
The roundings to bfloat16 on the way count: a program that leaves them out, or rounds other values in their place, can miss the bound.
Values may be sent and summed in bfloat16 or wider, within the bound.
A program may use at most 64 MiB of HBM per device.

v0:
```python
import math
import jax
import jax.numpy as jnp
from jax import lax
from jax.sharding import PartitionSpec as P

HD = 64
VD = 128
POOL_SPAN = 16
epsilon = 1e-06
very_low = -1e30


def extended(cells, sides, width):
    for axis, dim in sides:
        count = lax.axis_size(axis)
        ends = count - 1
        head = lax.slice_in_dim(cells, 0, width, axis=dim)
        tail = lax.slice_in_dim(cells, cells.shape[dim] - width, cells.shape[dim], axis=dim)
        cells = jnp.concatenate(
            [
                lax.ppermute(tail, axis, [(i, (i + 1) % count) for i in range(ends)]),
                cells,
                lax.ppermute(head, axis, [((i + 1) % count, i) for i in range(ends)]),
            ],
            axis=dim,
        )
    return cells


def add_products(totals, pieces, source):
    results = []
    for running, piece in zip(totals, pieces):
        results.append(jnp.dot(source, piece, preferred_element_type=jnp.float32))
    return tuple(results)


def on_device(
    tokens,
    norm_gain,
    query_weight,
    key_weight,
    value_weight,
    map_lambda,
    head_gain,
    attn_out_weight,
    pool_out_weight,
):
    tokens_wide = tokens.astype(jnp.float32)
    normed = (
        tokens_wide
        * lax.rsqrt(jnp.mean(tokens_wide * tokens_wide, axis=-1, keepdims=True) + epsilon)
        * norm_gain
    ).astype(jnp.bfloat16)
    row_count = normed.shape[0]
    sp_index = lax.axis_index("sp")
    tp_index = lax.axis_index("tp")
    group_width = pool_out_weight.shape[0]
    local_heads = map_lambda.shape[0]
    key_heads = value_weight.shape[1] // VD
    group_heads = local_heads // key_heads
    q_empty = jnp.zeros((row_count, query_weight.shape[1]), jnp.float32)
    k_empty = jnp.zeros((row_count, key_weight.shape[1]), jnp.float32)
    v_empty = jnp.zeros((row_count, value_weight.shape[1]), jnp.float32)
    q_acc, k_acc, v_acc = add_products(
        (q_empty, k_empty, v_empty),
        (
            lax.all_gather(query_weight, "sp", axis=0, tiled=True),
            lax.all_gather(key_weight, "sp", axis=0, tiled=True),
            lax.all_gather(value_weight, "sp", axis=0, tiled=True),
        ),
        normed,
    )
    queries = q_acc.astype(jnp.bfloat16).reshape(row_count, key_heads, group_heads, 2, HD)
    keys_flat = k_acc.astype(jnp.bfloat16)
    values_flat = v_acc.astype(jnp.bfloat16)

    def key_block(state_now, key_pair):
        maxima, totals, accums = state_now
        key_blk, val_blk = key_pair
        scores = jnp.einsum(
            "qhgmd,khmd->hgmqk", queries, key_blk, preferred_element_type=jnp.float32
        ) * HD ** (-0.5)
        highest = jnp.maximum(maxima, jnp.max(scores, axis=-1))
        factor = jnp.exp(maxima - highest)
        weights = jnp.exp(scores - highest[..., None])
        totals = totals * factor + jnp.sum(weights, axis=-1)
        accums = accums * factor[..., None] + jnp.einsum(
            "hgmqk,khe->hgmqe",
            weights.astype(jnp.bfloat16),
            val_blk,
            preferred_element_type=jnp.float32,
        )
        return ((highest, totals, accums), None)

    start_state = (
        jnp.full((key_heads, group_heads, 2, row_count), very_low, jnp.float32),
        jnp.zeros((key_heads, group_heads, 2, row_count), jnp.float32),
        jnp.zeros((key_heads, group_heads, 2, row_count, VD), jnp.float32),
    )
    key_piece = lax.all_gather(keys_flat, "sp", axis=0, tiled=True)
    val_piece = lax.all_gather(values_flat, "sp", axis=0, tiled=True)
    piece_len = key_piece.shape[0]
    block_len = math.gcd(piece_len, 512)
    key_blocks = key_piece.reshape(piece_len // block_len, block_len, key_heads, 2, HD)
    val_blocks = val_piece.reshape(piece_len // block_len, block_len, key_heads, VD)
    state_next, unused = lax.scan(key_block, start_state, (key_blocks, val_blocks))
    maxima, totals, accums = state_next
    log_parts = maxima + jnp.log(totals)
    log_totals = jnp.transpose(log_parts, (2, 0, 1, 3)).reshape(2, local_heads, row_count)
    reads = accums / totals[..., None]
    contrast = reads[:, :, 0] - map_lambda.reshape(key_heads, group_heads, 1, 1) * reads[:, :, 1]
    scaled = (
        contrast
        * lax.rsqrt(jnp.mean(contrast * contrast, axis=-1, keepdims=True) + epsilon)
        * head_gain.reshape(key_heads, group_heads, 1, VD)
    )
    attention_head_rows = (
        jnp.transpose(scaled, (2, 0, 1, 3))
        .reshape(row_count, local_heads * VD)
        .astype(jnp.bfloat16)
    )
    head_rows, log_totals = (attention_head_rows, log_totals)
    own_chan = lax.dynamic_slice_in_dim(normed, tp_index * group_width, group_width, 1)
    reach = POOL_SPAN // 2
    padded = extended(own_chan, (("sp", 0),), reach)
    window = jnp.left_shift(jnp.int32(2), tp_index)
    half_span = window // 2
    running = jnp.zeros((row_count, group_width), jnp.float32)
    for offset in range(POOL_SPAN):
        piece = lax.dynamic_slice_in_dim(padded, reach - half_span + offset, row_count, 0).astype(
            jnp.float32
        )
        running = running + jnp.where(offset < window, piece, 0.0)
    seq_len = row_count * lax.axis_size("sp")
    position = sp_index * row_count + jnp.arange(row_count, dtype=jnp.int32)
    lower_edge = jnp.clip(position - half_span, 0, seq_len)
    upper_edge = jnp.clip(position + window - half_span, 0, seq_len)
    counts_f = (upper_edge - lower_edge).astype(jnp.float32)[:, None]
    pooled = (running / counts_f - own_chan.astype(jnp.float32)).astype(jnp.bfloat16)
    attn_whole, pool_whole = (
        lax.all_gather(attn_out_weight, "sp", axis=1, tiled=True),
        lax.all_gather(pool_out_weight, "sp", axis=1, tiled=True),
    )
    mixed = lax.psum_scatter(
        (
            jnp.dot(head_rows, attn_whole, preferred_element_type=jnp.float32)
            + jnp.dot(pooled, pool_whole, preferred_element_type=jnp.float32)
        ).astype(jnp.bfloat16),
        "tp",
        scatter_dimension=0,
        tiled=True,
    )
    return (mixed, log_totals)


def solution(mesh):
    placed = (
        P(("grp", "sp"), None),
        P(),
        P("sp", "tp"),
        P("sp", "tp"),
        P("sp", "tp"),
        P("tp"),
        P("tp", None),
        P("tp", "sp"),
        P("tp", "sp"),
    )
    return jax.shard_map(
        on_device,
        mesh=mesh,
        in_specs=placed,
        out_specs=(P(("grp", "sp", "tp"), None), P(None, "tp", ("grp", "sp"))),
        check_vma=False,
    )
```

profile of v0, /device:TPU:0, one launch (start us, length us, event | category | flops | bytes accessed | tf_op | source)
XLA Modules:
  0.0 200.9 jit_solution(6198464641306412881)
XLA Ops:
  7.2 0.0 copy-start
  7.2 0.0 copy-start.1
  7.2 0.0 all-gather.4.cloned.1.call-start
  7.2 0.7 all-gather.4.cloned.1.call-update
  7.9 0.0 all-gather.6.cloned.1.call-start
  8.0 0.7 all-gather.6.cloned.1.call-update
  8.7 0.0 all-gather.8.cloned.1.call-start
  8.7 1.3 fusion.15
  10.0 0.0 copy-done
  10.0 0.0 copy-start.2
  10.0 1.0 fusion.17
  11.0 5.0 %collective-permute-start = (bf16[8,512]{1,0:T(8,128)(2,1)S(1)}, bf16[8,512]{1,0:T(8,128)(2,1)S(1)}, u32[]{:S(2)}, u32[]{:S(2)}) collective-permute-start(bf16[8,512]{1,0:T(8,128)(2,1)S(1)} %get-tuple-element.102), channel_id=1, source_target_pairs={{0,4},{4,8},{8,12},{1,5},{5,9},{9,13},{2,6},{6,10},{10,14},{3,7},{... | collective-permute-start | bytes 24584 | tf_op jit(solution)/shard_map/ppermute | solution.py:22
  16.0 1.3 collective-permute-start.1
  17.3 0.0 all-gather.8.cloned.1.call-update
  17.3 0.0 reduce-scatter.2.cloned.1.call-start
  17.4 0.0 copy-done.1
  17.4 24.1 %all_gather.21 = bf16[2048,128]{1,0:T(8,128)(2,1)S(1)} all-gather(bf16[512,128]{1,0:T(8,128)(2,1)S(1)} %copy-done.1), channel_id=1, replica_groups=mesh['grp'=2,'sp'=4,'tp'=4] {'sp'}, dimensions={0}, use_global_device_ids=true | all-gather | bytes 655360 | tf_op jit(solution)/shard_map/all_gather | solution.py:69
  41.5 0.3 convolution_convert_fusion.2
  41.9 15.2 %all_gather.22 = bf16[640,128]{1,0:T(8,128)(2,1)S(1)} all-gather(bf16[160,128]{1,0:T(8,128)(2,1)S(1)} %convolution_convert_fusion.2), channel_id=1, replica_groups=mesh['grp'=2,'sp'=4,'tp'=4] {'sp'}, dimensions={0}, use_global_device_ids=true | all-gather | bytes 204800 | tf_op jit(solution)/shard_map/all_gather | solution.py:101
  57.1 0.0 copy-done.2
  57.1 21.5 %all_gather.24 = bf16[2048,128]{1,0:T(8,128)(2,1)S(1)} all-gather(bf16[512,128]{1,0:T(8,128)(2,1)S(1)} %copy-done.2), channel_id=1, replica_groups=mesh['grp'=2,'sp'=4,'tp'=4] {'sp'}, dimensions={0}, use_global_device_ids=true | all-gather | bytes 655360 | tf_op jit(solution)/shard_map/all_gather | solution.py:70
  78.5 0.3 convolution_convert_fusion.1
  78.9 14.8 %all_gather.25 = bf16[640,128]{1,0:T(8,128)(2,1)S(1)} all-gather(bf16[160,128]{1,0:T(8,128)(2,1)S(1)} %convolution_convert_fusion.1), channel_id=1, replica_groups=mesh['grp'=2,'sp'=4,'tp'=4] {'sp'}, dimensions={0}, use_global_device_ids=true | all-gather | bytes 204800 | tf_op jit(solution)/shard_map/all_gather | solution.py:102
  93.7 0.2 reshape.142
  93.8 0.2 copy.22
  94.1 0.0 collective-permute-done
  94.2 0.0 collective-permute-done.1
  94.2 0.0 all-gather.4.cloned.1.call-done
  94.2 2.1 %convolution_convert_fusion = bf16[160,512]{1,0:T(8,128)(2,1)S(1)} fusion(bf16[160,2048]{1,0:T(8,128)(2,1)S(1)} %fusion.17, bf16[2048,512]{1,0:T(8,128)(2,1)} %all-gather.4.cloned.1.call-done), kind=kOutput, calls=%fused_computation.29 | convolution fusion | flops 335626240 | bytes 2916352 | tf_op jit(solution)/shard_map/dot_general | solution.py:34
  96.4 0.1 copy.21
  96.5 0.0 copy-start.4
  96.5 0.0 copy-start.3
  96.6 8.5 %while.15 = (s32[]{:T(128)}, f32[1,4,2,160]{3,1,2,0:T(4,128)S(1)}, f32[1,4,2,160]{3,1,2,0:T(4,128)S(1)}, f32[1,4,2,160,128]{4,3,2,1,0:T(8,128)S(1)}, bf16[5,128,...) while((s32[]{:T(128)}, f32[1,4,2,160]{3,1,2,0:T(4,128)S(1)}, ...), condition=%wide.region_4.5_spmd.clone, body=%wide.region_1.4_spmd.clone.sunk | while | flops 64232960 | bytes 3694705 | solution.py:107
  96.6 0.6 fusion.78
  97.2 0.6 fusion.80
  97.8 0.4 fusion.81
  98.3 0.6 fusion.78
  98.9 0.6 fusion.80
  99.5 0.4 fusion.81
  100.0 0.6 fusion.78
  100.6 0.6 fusion.80
  101.2 0.4 fusion.81
  101.7 0.6 fusion.78
  102.3 0.6 fusion.80
  102.9 0.4 fusion.81
  103.4 0.6 fusion.78
  104.0 0.6 fusion.80
  104.6 0.4 fusion.81
  105.1 0.2 broadcast_divide_fusion
  105.3 0.0 copy-done.4
  105.3 0.3 multiply_reduce_fusion
  105.6 0.0 copy-done.3
  105.6 0.2 fusion.20
  105.8 0.1 copy.27
  105.9 16.4 %all-gather.6.cloned.1.call-done = bf16[512,2048]{1,0:T(8,128)(2,1)} async-done(((bf16[512,512]{1,0:T(8,128)(2,1)}), bf16[512,2048]{1,0:T(8,128)(2,1)}) %all-gather.6.cloned.1.call-update) | async-done | bytes 2097168 | tf_op jit(solution)/shard_map/all_gather | solution.py:142
  122.4 2.1 %fusion.21 = f32[160,2048]{1,0:T(8,128)S(1)} fusion(bf16[512,2048]{1,0:T(8,128)(2,1)} %all-gather.6.cloned.1.call-done, bf16[20,8,4,128]{3,2,1,0:T(4,128)(2,1)S(1)} %bitcast.102), kind=kOutput, calls=%fused_computation.42 | convolution fusion | flops 335544320 | bytes 3571712 | tf_op jit(solution)/shard_map/dot_general | solution.py:147
  124.5 44.1 %all-gather.8.cloned.1.call-done = bf16[512,2048]{1,0:T(8,128)(2,1)} async-done(((bf16[512,512]{1,0:T(8,128)(2,1)}), bf16[512,2048]{1,0:T(8,128)(2,1)}) %all-gather.8.cloned.1.call-update) | async-done | bytes 2097168 | tf_op jit(solution)/shard_map/all_gather | solution.py:143
  168.6 4.3 %fusion.14 = bf16[160,2048]{1,0:T(8,128)(2,1)} fusion(f32[160,2048]{1,0:T(8,128)S(1)} %fusion.21, bf16[512,2048]{1,0:T(8,128)(2,1)} %all-gather.8.cloned.1.call-done, bf16[160,512]{1,0:T(8,128)(2,1)S(1)} %constant_dynamic-slice_fusion.1, f32[160]{0:T(256)S(1)} %subtract_convert_fusion.2, bf16[176,512]{1,0:T(8,128)(2,1)S(1)} %pad_maximum_fusion, ...), kind=kOutput, calls=%fused_computation.23 | convolution fusion | flops 340377600 | bytes 6849616 | tf_op jit(solution)/shard_map/dot_general | solution.py:148
  172.9 0.0 reduce-scatter.2.cloned.1.call-update
  172.9 0.6 add_bitcast_fusion
  173.5 20.8 %reduce-scatter.2.cloned.1.call-done = bf16[40,2048]{1,0:T(8,128)(2,1)} async-done(((bf16[160,2048]{1,0:T(8,128)(2,1)}), bf16[40,2048]{1,0:T(8,128)(2,1)}) %reduce-scatter.2.cloned.1.call-update) | async-done | bytes 163856 | tf_op jit(solution)/shard_map/reduce_scatter | solution.py:145
  (31 shorter events, 0.3 us)
Async XLA Ops:
  7.2 2.9 %copy-start = (bf16[160,2048]{1,0:T(8,128)(2,1)S(1)}, bf16[160,2048]{1,0:T(8,128)(2,1)}, u32[]{:S(2)}) copy-start(bf16[160,2048]{1,0:T(8,128)(2,1)} %param.11) | copy-start | bytes 1966084
  7.2 10.3 %copy-start.1 = (bf16[512,128]{1,0:T(8,128)(2,1)S(1)}, bf16[512,128]{1,0:T(8,128)(2,1)}, u32[]{:S(2)}) copy-start(bf16[512,128]{1,0:T(8,128)(2,1)} %param.14) | copy-start | bytes 393220
  7.2 87.0 %all-gather.4.cloned.1.call-start = ((), (), s32[]{:S(2)}) async-start(), calls=%async_computation.1 | async-start | bytes 2621440 | tf_op jit(solution)/shard_map/all_gather | solution.py:68
  7.9 114.4 %all-gather.6.cloned.1.call-start = ((), (), s32[]{:S(2)}) async-start(), calls=%async_computation.2 | async-start | bytes 2621440 | tf_op jit(solution)/shard_map/all_gather | solution.py:142
  8.7 159.9 %all-gather.8.cloned.1.call-start = ((), (), s32[]{:S(2)}) async-start(), calls=%async_computation.3 | async-start | bytes 2621440 | tf_op jit(solution)/shard_map/all_gather | solution.py:143
  10.0 47.0 %copy-start.2 = (bf16[512,128]{1,0:T(8,128)(2,1)S(1)}, bf16[512,128]{1,0:T(8,128)(2,1)}, u32[]{:S(2)}) copy-start(bf16[512,128]{1,0:T(8,128)(2,1)} %param.15) | copy-start | bytes 393220
  11.0 83.1 %collective-permute-start = (bf16[8,512]{1,0:T(8,128)(2,1)S(1)}, bf16[8,512]{1,0:T(8,128)(2,1)S(1)}, u32[]{:S(2)}, u32[]{:S(2)}) collective-permute-start(bf16[8,512]{1,0:T(8,128)(2,1)S(1)} %get-tuple-element.102), channel_id=1, source_target_pairs={{0,4},{4,8},{8,12},{1,5},{5,9},{9,13},{2,6},{6,10},{10,14},{3,7},{... | collective-permute-start | bytes 24584 | tf_op jit(solution)/shard_map/ppermute | solution.py:22
  16.0 78.2 %collective-permute-start.1 = (bf16[8,512]{1,0:T(8,128)(2,1)S(1)}, bf16[8,512]{1,0:T(8,128)(2,1)S(1)}, u32[]{:S(2)}, u32[]{:S(2)}) collective-permute-start(bf16[8,512]{1,0:T(8,128)(2,1)S(1)} %get-tuple-element.103), channel_id=1, source_target_pairs={{4,0},{8,4},{12,8},{5,1},{9,5},{13,9},{6,2},{10,6},{14,10},{7,3},{... | collective-permute-start | bytes 24584 | tf_op jit(solution)/shard_map/ppermute | solution.py:24
  17.3 177.0 %reduce-scatter.2.cloned.1.call-start = ((), (), s32[]{:S(2)}) async-start(), calls=%async_computation.4 | async-start | bytes 819200 | tf_op jit(solution)/shard_map/reduce_scatter | solution.py:145
  96.5 8.8 %copy-start.4 = (f32[4]{0:T(128)S(1)}, f32[4]{0:T(128)}, u32[]{:S(2)}) copy-start(f32[4]{0:T(128)} %param.16) | copy-start | bytes 52
  96.5 9.1 %copy-start.3 = (f32[4,128]{1,0:T(4,128)S(1)}, f32[4,128]{1,0:T(4,128)}, u32[]{:S(2)}) copy-start(f32[4,128]{1,0:T(4,128)} %param.17) | copy-start | bytes 6148
Sparse Core Ops, SparseCore 0:
  9.6 66.0 all-gather.3
  77.3 45.0 all-gather.5
  123.9 44.6 all-gather.7
  173.1 21.2 reduce-scatter.1
where the time goes:
time: 201 us
  waiting for transfers between devices  82.8 us (41%)
  blocking collectives  75.5 us (38%)
  matrix products  14.4 us (7%)
  between operations  14.2 us (7%)
  other arithmetic  6.68 us (3%)
  starting transfers between devices  6.4 us (3%)
    all_gather x1, waiting for transfers between devices, on_device(): lax.all_gather(pool_out_weight, 'sp', axis=1, tiled=True)  44.1 us
    all_gather x1, blocking collectives, on_device(): lax.all_gather(key_weight, 'sp', axis=0, tiled=True)  24.1 us
    all_gather x1, blocking collectives, on_device(): lax.all_gather(value_weight, 'sp', axis=0, tiled=True)  21.5 us
    reduce_scatter x1, waiting for transfers between devices, on_device(): lax.psum_scatter((jnp.dot(head_rows, attn_whole, preferred_element_type=j...  20.8 us
    all_gather x1, waiting for transfers between devices, on_device(): lax.all_gather(attn_out_weight, 'sp', axis=1, tiled=True)  16.4 us
    all_gather x1, blocking collectives, on_device(): key_piece = lax.all_gather(keys_flat, 'sp', axis=0, tiled=True)  15.2 us
    all_gather x1, blocking collectives, on_device(): val_piece = lax.all_gather(values_flat, 'sp', axis=0, tiled=True)  14.8 us
    ppermute x1, starting transfers between devices, extended(): lax.ppermute(tail, axis, [(i, (i + 1) % count) for i in range(ends)])  4.96 us
  transfers between devices with their start and end apart: 6, of which 3 were waited for; matrix products, arithmetic and copies ran while one was open for 9% of the time, Pallas kernels for 0%

commit v1 on v0

--- a/solution.py
+++ b/solution.py
@@ -98,7 +98,14 @@
         jnp.zeros((key_heads, group_heads, 2, row_count), jnp.float32),
         jnp.zeros((key_heads, group_heads, 2, row_count, VD), jnp.float32),
     )
-    key_piece = lax.all_gather(keys_flat, "sp", axis=0, tiled=True)
+    size = lax.axis_size("sp")
+    right = [(i_2, (i_2 + 1) % size) for i_2 in range(size)]
+    parts = [keys_flat]
+    for far in range(1, size):
+        parts = [lax.ppermute(parts[0], "sp", right), *parts]
+    result = jnp.concatenate(parts, axis=0)
+    turn = (lax.axis_index("sp") + 1) * parts[-1].shape[0]
+    key_piece = jnp.roll(result, turn, axis=0)
     val_piece = lax.all_gather(values_flat, "sp", axis=0, tiled=True)
     piece_len = key_piece.shape[0]
     block_len = math.gcd(piece_len, 512)

time: 201 us -> 199 us (0.990)
  blocking collectives: 75.5 us -> 61 us
  waiting for transfers between devices: 82.8 us -> 95.2 us
    all_gather x1 -> x0, blocking collectives: 15.2 us -> none  [on_device(): key_piece = lax.all_gather(keys_flat, 'sp', axis=0, tiled=True)]
    all_gather x1, waiting for transfers between devices: 16.4 us -> 24.1 us  [on_device(): lax.all_gather(attn_out_weight, 'sp', axis=1, tiled=True)]
    ppermute x0 -> x3, waiting for transfers between devices: none -> 4.83 us  [on_device(): parts = [lax.ppermute(parts[0], 'sp', right), *parts]]
    all_gather x1, blocking collectives: 21.5 us -> 24 us  [on_device(): lax.all_gather(value_weight, 'sp', axis=0, tiled=True)]
    ppermute x0 -> x3, starting transfers between devices: none -> 2.54 us  [on_device(): parts = [lax.ppermute(parts[0], 'sp', right), *parts]]
    ppermute x1, starting transfers between devices: 4.96 us -> 2.65 us  [extended(): lax.ppermute(tail, axis, [(i, (i + 1) % count) for i in range(ends)])]
    all_gather x1, blocking collectives: 24.1 us -> 22 us  [on_device(): lax.all_gather(key_weight, 'sp', axis=0, tiled=True)]
  transfers between devices with their start and end apart: 6 -> 9, of which waited for: 3 -> 4; matrix products, arithmetic and copies ran while one was open for 9% -> 8% of each run, Pallas kernels for 0% -> 0%
where the time goes in v1:
time: 199 us; the launch traced here: 198 us
  waiting for transfers between devices  95.2 us (48%)
  blocking collectives  61 us (31%)
  matrix products  14.3 us (7%)
  between operations  14.1 us (7%)
  starting transfers between devices  6.64 us (3%)
  other arithmetic  5.95 us (3%)
    all_gather x1, waiting for transfers between devices, on_device(): lax.all_gather(pool_out_weight, 'sp', axis=1, tiled=True)  44 us
    all_gather x1, waiting for transfers between devices, on_device(): lax.all_gather(attn_out_weight, 'sp', axis=1, tiled=True)  24.1 us
    all_gather x1, blocking collectives, on_device(): lax.all_gather(value_weight, 'sp', axis=0, tiled=True)  24 us
    all_gather x1, blocking collectives, on_device(): lax.all_gather(key_weight, 'sp', axis=0, tiled=True)  22 us
    reduce_scatter x1, waiting for transfers between devices, on_device(): lax.psum_scatter((jnp.dot(head_rows, attn_whole, preferred_element_type=j...  20.8 us
    all_gather x1, blocking collectives, on_device(): val_piece = lax.all_gather(values_flat, 'sp', axis=0, tiled=True)  14.9 us
    ppermute x3, waiting for transfers between devices, on_device(): parts = [lax.ppermute(parts[0], 'sp', right), *parts]  4.83 us
    dot_general x1, matrix products, on_device(): jnp.dot(pooled, pool_whole, preferred_element_type=jnp.float32)  4.32 us
  transfers between devices with their start and end apart: 9, of which 4 were waited for; matrix products, arithmetic and copies ran while one was open for 8% of the time, Pallas kernels for 0%

profile of v1, /device:TPU:0, one launch (start us, length us, event | category | flops | bytes accessed | tf_op | source)
XLA Modules:
  0.0 198.2 jit_solution(13286622720465916657)
XLA Ops:
  7.2 0.0 copy-start
  7.2 0.0 copy-start.2
  7.2 0.0 all-gather.4.cloned.1.call-start
  7.2 0.7 all-gather.4.cloned.1.call-update
  7.9 0.0 all-gather.6.cloned.1.call-start
  8.0 0.7 all-gather.6.cloned.1.call-update
  8.7 0.0 all-gather.8.cloned.1.call-start
  8.7 1.3 fusion.15
  10.0 22.0 %all_gather.18 = bf16[2048,128]{1,0:T(8,128)(2,1)S(1)} all-gather(bf16[512,128]{1,0:T(8,128)(2,1)} %param.14), channel_id=1, replica_groups=mesh['grp'=2,'sp'=4,'tp'=4] {'sp'}, dimensions={0}, use_global_device_ids=true | all-gather | bytes 655360 | tf_op jit(solution)/shard_map/all_gather | solution.py:69
  32.0 0.0 copy-done
  32.0 0.0 copy-done.2
  32.1 0.2 fusion.17
  32.3 0.3 convolution_convert_fusion.2
  32.6 0.9 collective-permute-start
  33.6 2.7 %collective-permute-start.3 = (bf16[8,512]{1,0:T(8,128)(2,1)S(1)}, bf16[8,512]{1,0:T(8,128)(2,1)S(1)}, u32[]{:S(2)}, u32[]{:S(2)}) collective-permute-start(bf16[8,512]{1,0:T(8,128)(2,1)S(1)} %get-tuple-element.102), channel_id=1, source_target_pairs={{0,4},{4,8},{8,12},{1,5},{5,9},{9,13},{2,6},{6,10},{10,14},{3,7},{... | collective-permute-start | bytes 24584 | tf_op jit(solution)/shard_map/ppermute | solution.py:22
  36.2 1.3 collective-permute-start.4
  37.5 0.0 all-gather.8.cloned.1.call-update
  37.5 0.0 reduce-scatter.2.cloned.1.call-start
  37.6 24.0 %all_gather.20 = bf16[2048,128]{1,0:T(8,128)(2,1)S(1)} all-gather(bf16[512,128]{1,0:T(8,128)(2,1)S(1)} %copy-done.1), channel_id=1, replica_groups=mesh['grp'=2,'sp'=4,'tp'=4] {'sp'}, dimensions={0}, use_global_device_ids=true | all-gather | bytes 655360 | tf_op jit(solution)/shard_map/all_gather | solution.py:70
  61.7 0.3 convolution_convert_fusion.1
  62.1 0.0 collective-permute-done
  62.1 0.6 collective-permute-start.1
  62.7 14.9 %all_gather.21 = bf16[640,128]{1,0:T(8,128)(2,1)S(1)} all-gather(bf16[160,128]{1,0:T(8,128)(2,1)S(1)} %convolution_convert_fusion.1), channel_id=1, replica_groups=mesh['grp'=2,'sp'=4,'tp'=4] {'sp'}, dimensions={0}, use_global_device_ids=true | all-gather | bytes 204800 | tf_op jit(solution)/shard_map/all_gather | solution.py:109
  77.6 0.0 collective-permute-done.1
  77.6 1.0 collective-permute-start.2
  78.6 0.0 collective-permute-done.3
  78.6 0.0 collective-permute-done.4
  78.6 4.8 %collective-permute-done.2 = bf16[160,128]{1,0:T(8,128)(2,1)S(1)} collective-permute-done((bf16[160,128]{1,0:T(8,128)(2,1)S(1)}, bf16[160,128]{1,0:T(8,128)(2,1)S(1)}, u32[]{:S(2)}, u32[]{:S(2)}) %collective-permute-start.2) | collective-permute-done | bytes 40992 | tf_op jit(solution)/shard_map/ppermute | solution.py:105
  83.6 0.1 constant_dynamic-slice_fusion.2
  83.6 0.1 reshape.142
  83.8 0.2 copy.21
  84.0 0.0 all-gather.4.cloned.1.call-done
  84.0 2.1 %convolution_convert_fusion = bf16[160,512]{1,0:T(8,128)(2,1)S(1)} fusion(bf16[160,2048]{1,0:T(8,128)(2,1)S(1)} %fusion.17, bf16[2048,512]{1,0:T(8,128)(2,1)} %all-gather.4.cloned.1.call-done), kind=kOutput, calls=%fused_computation.29 | convolution fusion | flops 335626240 | bytes 2916352 | tf_op jit(solution)/shard_map/dot_general | solution.py:34
  86.1 0.1 copy.20
  86.3 0.0 copy-start.4
  86.3 0.0 copy-start.3
  86.3 8.5 %while.15 = (s32[]{:T(128)}, f32[1,4,2,160]{3,1,2,0:T(4,128)S(1)}, f32[1,4,2,160]{3,1,2,0:T(4,128)S(1)}, f32[1,4,2,160,128]{4,3,2,1,0:T(8,128)S(1)}, bf16[5,128,...) while((s32[]{:T(128)}, f32[1,4,2,160]{3,1,2,0:T(4,128)S(1)}, ...), condition=%wide.region_4.5_spmd.clone, body=%wide.region_1.4_spmd.clone.sunk | while | flops 64232960 | bytes 3694705 | solution.py:114
  86.3 0.6 fusion.78
  87.0 0.6 fusion.80
  87.6 0.4 fusion.81
  88.0 0.6 fusion.78
  88.7 0.6 fusion.80
  89.3 0.4 fusion.81
  89.7 0.6 fusion.78
  90.4 0.6 fusion.80
  91.0 0.4 fusion.81
  91.4 0.6 fusion.78
  92.1 0.6 fusion.80
  92.7 0.4 fusion.81
  93.1 0.6 fusion.78
  93.8 0.6 fusion.80
  94.4 0.4 fusion.81
  94.9 0.2 broadcast_divide_fusion
  95.1 0.0 copy-done.4
  95.1 0.3 multiply_reduce_fusion
  95.4 0.2 fusion.20
  95.6 0.1 copy.26
  95.7 24.1 %all-gather.6.cloned.1.call-done = bf16[512,2048]{1,0:T(8,128)(2,1)} async-done(((bf16[512,512]{1,0:T(8,128)(2,1)}), bf16[512,2048]{1,0:T(8,128)(2,1)}) %all-gather.6.cloned.1.call-update) | async-done | bytes 2097168 | tf_op jit(solution)/shard_map/all_gather | solution.py:149
  119.8 2.1 %fusion.21 = f32[160,2048]{1,0:T(8,128)S(1)} fusion(bf16[512,2048]{1,0:T(8,128)(2,1)} %all-gather.6.cloned.1.call-done, bf16[20,8,4,128]{3,2,1,0:T(4,128)(2,1)S(1)} %bitcast.102), kind=kOutput, calls=%fused_computation.42 | convolution fusion | flops 335544320 | bytes 3571712 | tf_op jit(solution)/shard_map/dot_general | solution.py:154
  121.9 44.0 %all-gather.8.cloned.1.call-done = bf16[512,2048]{1,0:T(8,128)(2,1)} async-done(((bf16[512,512]{1,0:T(8,128)(2,1)}), bf16[512,2048]{1,0:T(8,128)(2,1)}) %all-gather.8.cloned.1.call-update) | async-done | bytes 2097168 | tf_op jit(solution)/shard_map/all_gather | solution.py:150
  165.9 4.3 %fusion.14 = bf16[160,2048]{1,0:T(8,128)(2,1)} fusion(f32[160,2048]{1,0:T(8,128)S(1)} %fusion.21, bf16[512,2048]{1,0:T(8,128)(2,1)} %all-gather.8.cloned.1.call-done, bf16[160,512]{1,0:T(8,128)(2,1)S(1)} %constant_dynamic-slice_fusion.1, f32[160]{0:T(256)S(1)} %subtract_convert_fusion.2, bf16[176,512]{1,0:T(8,128)(2,1)S(1)} %pad_maximum_fusion, ...), kind=kOutput, calls=%fused_computation.23 | convolution fusion | flops 340377600 | bytes 6849616 | tf_op jit(solution)/shard_map/dot_general | solution.py:155
  170.2 0.0 reduce-scatter.2.cloned.1.call-update
  170.3 0.6 add_bitcast_fusion
  170.9 20.8 %reduce-scatter.2.cloned.1.call-done = bf16[40,2048]{1,0:T(8,128)(2,1)} async-done(((bf16[160,2048]{1,0:T(8,128)(2,1)}), bf16[40,2048]{1,0:T(8,128)(2,1)}) %reduce-scatter.2.cloned.1.call-update) | async-done | bytes 163856 | tf_op jit(solution)/shard_map/reduce_scatter | solution.py:152
  (42 shorter events, 0.4 us)
Async XLA Ops:
  7.2 24.9 %copy-start = (bf16[160,2048]{1,0:T(8,128)(2,1)S(1)}, bf16[160,2048]{1,0:T(8,128)(2,1)}, u32[]{:S(2)}) copy-start(bf16[160,2048]{1,0:T(8,128)(2,1)} %param.11) | copy-start | bytes 1966084
  7.2 24.9 %copy-start.2 = (f32[2048]{0:T(1024)S(1)}, f32[2048]{0:T(1024)}, u32[]{:S(2)}) copy-start(f32[2048]{0:T(1024)} %param.12) | copy-start | bytes 24580
  7.2 76.8 %all-gather.4.cloned.1.call-start = ((), (), s32[]{:S(2)}) async-start(), calls=%async_computation.1 | async-start | bytes 2621440 | tf_op jit(solution)/shard_map/all_gather | solution.py:68
  7.9 111.9 %all-gather.6.cloned.1.call-start = ((), (), s32[]{:S(2)}) async-start(), calls=%async_computation.2 | async-start | bytes 2621440 | tf_op jit(solution)/shard_map/all_gather | solution.py:149
  8.7 157.2 %all-gather.8.cloned.1.call-start = ((), (), s32[]{:S(2)}) async-start(), calls=%async_computation.3 | async-start | bytes 2621440 | tf_op jit(solution)/shard_map/all_gather | solution.py:150
  10.0 27.6 %copy-start.1 = (bf16[512,128]{1,0:T(8,128)(2,1)S(1)}, bf16[512,128]{1,0:T(8,128)(2,1)}, u32[]{:S(2)}) copy-start(bf16[512,128]{1,0:T(8,128)(2,1)} %param.15) | copy-start | bytes 393220
  32.6 29.5 %collective-permute-start = (bf16[160,128]{1,0:T(8,128)(2,1)S(1)}, bf16[160,128]{1,0:T(8,128)(2,1)S(1)}, u32[]{:S(2)}, u32[]{:S(2)}) collective-permute-start(bf16[160,128]{1,0:T(8,128)(2,1)S(1)} %convolution_convert_fusion.2), channel_id=1, source_target_pairs={{0,4},{4,8},{8,12},{12,0},{1,5},{5,9},{9,13},{13,1},{2,6},{6,10},{... | collective-permute-start | bytes 122888 | tf_op jit(solution)/shard_map/ppermute | solution.py:105
  33.6 45.0 %collective-permute-start.3 = (bf16[8,512]{1,0:T(8,128)(2,1)S(1)}, bf16[8,512]{1,0:T(8,128)(2,1)S(1)}, u32[]{:S(2)}, u32[]{:S(2)}) collective-permute-start(bf16[8,512]{1,0:T(8,128)(2,1)S(1)} %get-tuple-element.102), channel_id=1, source_target_pairs={{0,4},{4,8},{8,12},{1,5},{5,9},{9,13},{2,6},{6,10},{10,14},{3,7},{... | collective-permute-start | bytes 24584 | tf_op jit(solution)/shard_map/ppermute | solution.py:22
  36.2 42.4 %collective-permute-start.4 = (bf16[8,512]{1,0:T(8,128)(2,1)S(1)}, bf16[8,512]{1,0:T(8,128)(2,1)S(1)}, u32[]{:S(2)}, u32[]{:S(2)}) collective-permute-start(bf16[8,512]{1,0:T(8,128)(2,1)S(1)} %get-tuple-element.103), channel_id=1, source_target_pairs={{4,0},{8,4},{12,8},{5,1},{9,5},{13,9},{6,2},{10,6},{14,10},{7,3},{... | collective-permute-start | bytes 24584 | tf_op jit(solution)/shard_map/ppermute | solution.py:24
  37.5 154.1 %reduce-scatter.2.cloned.1.call-start = ((), (), s32[]{:S(2)}) async-start(), calls=%async_computation.4 | async-start | bytes 819200 | tf_op jit(solution)/shard_map/reduce_scatter | solution.py:152
  62.1 15.5 %collective-permute-start.1 = (bf16[160,128]{1,0:T(8,128)(2,1)S(1)}, bf16[160,128]{1,0:T(8,128)(2,1)S(1)}, u32[]{:S(2)}, u32[]{:S(2)}) collective-permute-start(bf16[160,128]{1,0:T(8,128)(2,1)S(1)} %collective-permute-done), channel_id=1, source_target_pairs={{0,4},{4,8},{8,12},{12,0},{1,5},{5,9},{9,13},{13,1},{2,6},{6,10},{... | collective-permute-start | bytes 122888 | tf_op jit(solution)/shard_map/ppermute | solution.py:105
  77.6 5.8 %collective-permute-start.2 = (bf16[160,128]{1,0:T(8,128)(2,1)S(1)}, bf16[160,128]{1,0:T(8,128)(2,1)S(1)}, u32[]{:S(2)}, u32[]{:S(2)}) collective-permute-start(bf16[160,128]{1,0:T(8,128)(2,1)S(1)} %collective-permute-done.1), channel_id=1, source_target_pairs={{0,4},{4,8},{8,12},{12,0},{1,5},{5,9},{9,13},{13,1},{2,6},{6,10},{... | collective-permute-start | bytes 122888 | tf_op jit(solution)/shard_map/ppermute | solution.py:105
  86.3 8.8 %copy-start.4 = (f32[4]{0:T(128)S(1)}, f32[4]{0:T(128)}, u32[]{:S(2)}) copy-start(f32[4]{0:T(128)} %param.16) | copy-start | bytes 52
  86.3 9.1 %copy-start.3 = (f32[4,128]{1,0:T(4,128)S(1)}, f32[4,128]{1,0:T(4,128)}, u32[]{:S(2)}) copy-start(f32[4,128]{1,0:T(4,128)} %param.17) | copy-start | bytes 6148
Sparse Core Ops, SparseCore 0:
  9.6 63.5 all-gather.3
  74.7 45.0 all-gather.5
  121.4 44.5 all-gather.7
  170.4 21.2 reduce-scatter.1
